TPU v7x, 32 devices: a whole 2x2x4 slice. The times are simulated.
32 devices in a mesh: grp: 2 (over y), sp: 4 (over z), tp: 4 (over x, core).
Axes of the slice: x: 2, y: 2, z: 4, core: 2. Of those that a mesh axis runs over, the one named last changes fastest.
Arguments:
- query_first: bfloat16 [1536, 512], P(('grp', 'sp'), 'tp'), parts along dimension 0, may hold values from -172 to 172
- key_first: bfloat16 [1536, 512], P(('grp', 'sp'), 'tp'), parts along dimension 0, may hold values from -7.8 to 7.8
- query_second: bfloat16 [1536, 1024], P(('grp', 'sp'), 'tp'), parts along dimension 0, may hold values from -172 to 172
- key_second: bfloat16 [1536, 1024], P(('grp', 'sp'), 'tp'), parts along dimension 0, may hold values from -7.8 to 7.8
- values: bfloat16 [1536, 2, 512], P(('grp', 'sp'), None, 'tp'), parts along dimension 0, may hold values from -6 to 6
- lambdas: float32 [2, 4], P(None, 'tp'), may hold values from 0.3 to 0.8
- residual: bfloat16 [1536, 2048], P(('grp', 'sp'), 'tp'), parts along dimension 0, may hold values from -130 to 130
- norm_gain: bfloat16 [2048], P('tp'), may hold values from 0.099609375 to 1.8984375
- out_weight: bfloat16 [2, 512, 2048], P(None, 'tp'), may hold values from -0.1875 to 0.1875
- gate_weight: bfloat16 [2048, 5632], P('sp', 'tp'), may hold values from -0.125 to 0.125
- up_weight: bfloat16 [2048, 5632], P('sp', 'tp'), may hold values from -0.125 to 0.125
- down_weight: bfloat16 [5632, 2048], P('tp', 'sp'), may hold values from -0.078125 to 0.078125
Outputs:
- layer_out: bfloat16 [1536, 2048], P(('grp', 'sp'), 'tp'), parts along dimension 0
There are 2 independent parts, one for each index of `grp`. A program takes and returns all parts, laid end to end along the dimension named above; an argument that names none is the same for every part. Nothing has to cross between parts.
All inputs are finite; a program needn't handle non-finite values.
Results may differ from a plain program's by a relative error of at most 0.0065.
Values may be sent and summed in bfloat16 or wider, within the bound.
A program may use at most 128 MiB of HBM per device.

v0:
```python
import jax
import jax.numpy as jnp
from jax import lax
from jax.sharding import PartitionSpec as P

D = 2048


def per_device(
    query_first,
    key_first,
    query_second,
    key_second,
    values,
    lambdas,
    residual,
    norm_gain,
    out_weight,
    gate_weight,
    up_weight,
    down_weight,
):
    tok_rows = query_first.shape[0]
    heads_here = lambdas.shape[1]
    width_first = query_first.shape[1] // (2 * heads_here)
    width_second = query_second.shape[1] // (2 * heads_here)
    value_size = values.shape[2] // heads_here
    offset = lax.axis_index("sp") * tok_rows
    query_pos = offset + lax.broadcasted_iota(jnp.int32, (tok_rows, 1), 0)
    query_groups = (
        query_first.reshape(tok_rows, heads_here, 2, width_first),
        query_second.reshape(tok_rows, heads_here, 2, width_second),
    )
    key_widths = (width_first, width_second)
    start_state = (
        jnp.full((heads_here, 2, tok_rows, 1), -1e30, jnp.float32),
        jnp.zeros((heads_here, 2, tok_rows, 1), jnp.float32),
        jnp.zeros((heads_here, 2, tok_rows, value_size), jnp.float32),
    )
    states = (start_state, start_state)
    pieces = (
        lax.all_gather(key_first, "sp", axis=0, tiled=True),
        lax.all_gather(key_second, "sp", axis=0, tiled=True),
        lax.all_gather(values, "sp", axis=0, tiled=True),
    )
    piece_rows = pieces[0].shape[0]
    key_pos = lax.broadcasted_iota(jnp.int32, (1, piece_rows), 1)
    allowed = key_pos <= query_pos
    value_rows = pieces[2].reshape(piece_rows, 2, heads_here, value_size)
    results = []
    for group_idx in range(2):
        key_width = key_widths[group_idx]
        key_part = pieces[group_idx].reshape(piece_rows, heads_here, 2, key_width)
        scores = jnp.einsum(
            "qhmd,khmd->hmqk", query_groups[group_idx], key_part, preferred_element_type=jnp.float32
        ) * key_width ** (-0.5)
        scores = jnp.where(allowed, scores, -1e30)
        running, totals, weighted = states[group_idx]
        new_peak = jnp.maximum(running, jnp.max(scores, axis=-1, keepdims=True))
        weights = jnp.where(allowed, jnp.exp(scores - new_peak), 0.0)
        totals = jnp.sum(weights, axis=-1, keepdims=True)
        weighted = jnp.einsum(
            "hmqk,khe->hmqe",
            weights.astype(jnp.bfloat16),
            value_rows[:, group_idx],
            preferred_element_type=jnp.float32,
        )
        results.append((new_peak, totals, weighted))
    states = (results[0], results[1])
    map_out = jnp.stack([states[0][2] / states[0][1], states[1][2] / states[1][1]])
    differ = map_out[:, :, 0] - lambdas[:, :, None, None] * map_out[:, :, 1]
    head_scale = lax.rsqrt(jnp.mean(differ * differ, axis=-1, keepdims=True) + 1e-06)
    attended = (0.8 * differ * head_scale).astype(jnp.bfloat16)
    projection = out_weight.reshape(2, heads_here, value_size, out_weight.shape[2])
    mixed_part = jnp.einsum(
        "ghqe,gher->qr", attended, projection, preferred_element_type=jnp.float32
    )
    mixed = lax.psum_scatter(
        mixed_part.astype(jnp.bfloat16), "tp", scatter_dimension=1, tiled=True
    ).astype(jnp.float32)
    stream = residual.astype(jnp.float32) + mixed
    squares = lax.psum(jnp.sum(stream * stream, axis=1), "tp")
    row_scale = lax.rsqrt(squares[:, None] / D + 1e-06)
    normed = (stream * row_scale * norm_gain.astype(jnp.float32)).astype(jnp.bfloat16)
    full_rows = lax.all_gather(normed, "tp", axis=1, tiled=True)
    pieces = (
        lax.all_gather(gate_weight, "sp", axis=0, tiled=True),
        lax.all_gather(up_weight, "sp", axis=0, tiled=True),
    )
    gate = jnp.dot(full_rows, pieces[0], preferred_element_type=jnp.float32)
    up_part = jnp.dot(full_rows, pieces[1], preferred_element_type=jnp.float32)
    hidden = (jax.nn.silu(gate) * up_part).astype(jnp.bfloat16)
    partial_out = jnp.dot(
        hidden,
        lax.all_gather(down_weight, "sp", axis=1, tiled=True),
        preferred_element_type=jnp.float32,
    )
    ffn = lax.psum_scatter(
        partial_out.astype(jnp.bfloat16), "tp", scatter_dimension=1, tiled=True
    ).astype(jnp.float32)
    return (stream + 0.5 * ffn).astype(jnp.bfloat16)


def solution(mesh):
    return jax.shard_map(
        per_device,
        mesh=mesh,
        in_specs=(
            P(("grp", "sp"), "tp"),
            P(("grp", "sp"), "tp"),
            P(("grp", "sp"), "tp"),
            P(("grp", "sp"), "tp"),
            P(("grp", "sp"), None, "tp"),
            P(None, "tp"),
            P(("grp", "sp"), "tp"),
            P("tp"),
            P(None, "tp", None),
            P("sp", "tp"),
            P("sp", "tp"),
            P("tp", "sp"),
        ),
        out_specs=P(("grp", "sp"), "tp"),
        check_vma=False,
    )
```

profile of v0, /device:TPU:0, one launch (start us, length us, event | category | flops | bytes accessed | tf_op | source)
XLA Modules:
  0.0 419.4 jit_solution(9682786560967322755)
XLA Ops:
  7.6 16.6 %all_gather.23 = bf16[768,256]{1,0:T(8,128)(2,1)S(1)} all-gather(bf16[192,256]{1,0:T(8,128)(2,1)} %param.15), channel_id=1, replica_groups=mesh['grp'=2,'sp'=4,'tp'=4] {'sp'}, dimensions={0}, use_global_device_ids=true | all-gather | bytes 491520 | tf_op jit(solution)/shard_map/all_gather | solution.py:43
  24.4 14.4 %all_gather.21 = bf16[768,128]{1,0:T(8,128)(2,1)S(1)} all-gather(bf16[192,128]{1,0:T(8,128)(2,1)S(1)} %copy-done.6), channel_id=1, replica_groups=mesh['grp'=2,'sp'=4,'tp'=4] {'sp'}, dimensions={0}, use_global_device_ids=true | all-gather | bytes 245760 | tf_op jit(solution)/shard_map/all_gather | solution.py:42
  39.1 14.8 %all_gather.22 = bf16[768,2,128]{2,0,1:T(8,128)(2,1)S(1)} all-gather(bf16[192,2,128]{2,0,1:T(8,128)(2,1)S(1)} %copy.27), channel_id=1, replica_groups=mesh['grp'=2,'sp'=4,'tp'=4] {'sp'}, dimensions={0}, use_global_device_ids=true | all-gather | bytes 491520 | tf_op jit(solution)/shard_map/all_gather | solution.py:44
  53.8 0.5 fusion.34
  54.3 0.5 fusion.35
  54.8 0.7 fusion.6
  55.5 0.4 fusion.5
  55.9 0.4 fusion.4
  56.8 1.3 fusion
  58.3 0.5 all-gather.4.cloned.1.call-update
  58.9 0.5 all-gather.6.cloned.1.call-update
  59.4 0.5 all-gather.8.cloned.1.call-update
  60.0 22.8 %reduce-scatter.3.cloned.1.call-done = bf16[192,512]{1,0:T(8,128)(2,1)} async-done(((bf16[192,2048]{1,0:T(8,128)(2,1)}), bf16[192,512]{1,0:T(8,128)(2,1)}) %reduce-scatter.3.cloned.1.call-update) | async-done | bytes 196624 | tf_op jit(solution)/shard_map/reduce_scatter | solution.py:78
  82.8 1.1 multiply_reduce_fusion
  83.9 6.1 %psum.7 = f32[192]{0:T(256)S(1)} all-reduce(f32[192]{0:T(256)S(1)} %multiply_reduce_fusion), channel_id=1, replica_groups=mesh['grp'=2,'sp'=4,'tp'=4] {'tp'}, use_global_device_ids=true, to_apply=%region_7.8 | all-reduce | flops 192 | bytes 1536 | tf_op jit(solution)/shard_map/psum | solution.py:82
  90.0 1.0 multiply_convert_fusion
  91.0 8.4 %all_gather.24 = bf16[192,2048]{1,0:T(8,128)(2,1)S(1)} all-gather(bf16[192,512]{1,0:T(8,128)(2,1)S(1)} %multiply_convert_fusion), channel_id=1, replica_groups=mesh['grp'=2,'sp'=4,'tp'=4] {'tp'}, dimensions={1}, use_global_device_ids=true | all-gather | bytes 983040 | tf_op jit(solution)/shard_map/all_gather | solution.py:85
  99.4 68.7 %all-gather.4.cloned.1.call-done = bf16[2048,1408]{1,0:T(8,128)(2,1)} async-done(((bf16[512,1408]{1,0:T(8,128)(2,1)}), bf16[2048,1408]{1,0:T(8,128)(2,1)}) %all-gather.4.cloned.1.call-update) | async-done | bytes 5767184 | tf_op jit(solution)/shard_map/all_gather | solution.py:87
  168.1 4.0 fusion.36
  172.1 102.2 %all-gather.6.cloned.1.call-done = bf16[2048,1408]{1,0:T(8,128)(2,1)} async-done(((bf16[512,1408]{1,0:T(8,128)(2,1)}), bf16[2048,1408]{1,0:T(8,128)(2,1)}) %all-gather.6.cloned.1.call-update) | async-done | bytes 5767184 | tf_op jit(solution)/shard_map/all_gather | solution.py:88
  274.4 106.3 %all-gather.8.cloned.1.call-done = bf16[1408,2048]{1,0:T(8,128)(2,1)} async-done(((bf16[1408,512]{1,0:T(8,128)(2,1)}), bf16[1408,2048]{1,0:T(8,128)(2,1)}) %all-gather.8.cloned.1.call-update) | async-done | bytes 5767184 | tf_op jit(solution)/shard_map/all_gather | solution.py:95
  380.6 7.9 %convolution_convert_fusion = bf16[192,2048]{1,0:T(8,128)(2,1)} fusion(bf16[1408,2048]{1,0:T(8,128)(2,1)} %all-gather.8.cloned.1.call-done, bf16[192,2048]{1,0:T(8,128)(2,1)S(1)} %all_gather.24, bf16[2048,1408]{1,0:T(8,128)(2,1)} %all-gather.6.cloned.1.call-done, f32[192,1408]{1,0:T(8,128)S(1)} %fusion.36), kind=kOutput, calls=%fused_computation.4 | convolution fusion | flops 2216607744 | bytes 14188544 | tf_op jit(solution)/shard_map/dot_general | solution.py:93
  388.5 21.6 %reduce-scatter.5.cloned.1.call-done = bf16[192,512]{1,0:T(8,128)(2,1)} async-done(((bf16[192,2048]{1,0:T(8,128)(2,1)}), bf16[192,512]{1,0:T(8,128)(2,1)}) %reduce-scatter.5.cloned.1.call-update) | async-done | bytes 196624 | tf_op jit(solution)/shard_map/reduce_scatter | solution.py:98
  410.2 1.7 add_convert_fusion
  (36 shorter events, 1.3 us)
Async XLA Ops:
  7.4 49.5 %copy-start = (bf16[2,128,2048]{2,1,0:T(8,128)(2,1)S(1)}, bf16[2,128,2048]{2,1,0:T(8,128)(2,1)}, u32[]{:S(2)}) copy-start(bf16[2,128,2048]{2,1,0:T(8,128)(2,1)} %param.20) | copy-start | bytes 3145732
  7.4 17.0 %copy-start.6 = (bf16[192,128]{1,0:T(8,128)(2,1)S(1)}, bf16[192,128]{1,0:T(8,128)(2,1)}, u32[]{:S(2)}) copy-start(bf16[192,128]{1,0:T(8,128)(2,1)} %param.13) | copy-start | bytes 147460
  7.4 31.5 %copy-start.5 = (bf16[192,128]{1,0:T(8,128)(2,1)S(1)}, bf16[192,128]{1,0:T(8,128)(2,1)}, u32[]{:S(2)}) copy-start(bf16[192,128]{1,0:T(8,128)(2,1)} %param.12) | copy-start | bytes 147460
  7.4 31.7 %copy-start.4 = (bf16[192,2,128]{2,1,0:T(2,128)(2,1)S(1)}, bf16[192,2,128]{2,1,0:T(2,128)(2,1)}, u32[]{:S(2)}) copy-start(bf16[192,2,128]{2,1,0:T(2,128)(2,1)} %param.16) | copy-start | bytes 294916
  7.4 75.4 %reduce-scatter.3.cloned.1.call-start = ((), (), s32[]{:S(2)}) async-start(), calls=%async_computation.2 | async-start | bytes 983040 | tf_op jit(solution)/shard_map/reduce_scatter | solution.py:78
  24.2 29.6 %copy-start.3 = (bf16[192,256]{1,0:T(8,128)(2,1)S(1)}, bf16[192,256]{1,0:T(8,128)(2,1)}, u32[]{:S(2)}) copy-start(bf16[192,256]{1,0:T(8,128)(2,1)} %param.14) | copy-start | bytes 294916
  55.9 0.7 copy-start.7
  58.2 109.9 %all-gather.4.cloned.1.call-start = ((), (), s32[]{:S(2)}) async-start(), calls=%async_computation.3 | async-start | bytes 7208960 | tf_op jit(solution)/shard_map/all_gather | solution.py:87
  58.8 1.2 copy-start.8
  58.8 24.0 %copy-start.1 = (bf16[192,512]{1,0:T(8,128)(2,1)S(1)}, bf16[192,512]{1,0:T(8,128)(2,1)}, u32[]{:S(2)}) copy-start(bf16[192,512]{1,0:T(8,128)(2,1)} %param.18) | copy-start | bytes 589828
  58.8 215.6 %all-gather.6.cloned.1.call-start = ((), (), s32[]{:S(2)}) async-start(), calls=%async_computation.4 | async-start | bytes 7208960 | tf_op jit(solution)/shard_map/all_gather | solution.py:88
  59.4 321.3 %all-gather.8.cloned.1.call-start = ((), (), s32[]{:S(2)}) async-start(), calls=%async_computation.5 | async-start | bytes 7208960 | tf_op jit(solution)/shard_map/all_gather | solution.py:95
  60.0 350.2 %reduce-scatter.5.cloned.1.call-start = ((), (), s32[]{:S(2)}) async-start(), calls=%async_computation.6 | async-start | bytes 983040 | tf_op jit(solution)/shard_map/reduce_scatter | solution.py:98
  172.1 238.0 %copy-start.2 = (bf16[192,512]{1,0:T(8,128)(2,1)S(1)}, bf16[192,512]{1,0:T(8,128)(2,1)}, u32[]{:S(2)}) copy-start(bf16[192,512]{1,0:T(8,128)(2,1)} %reduce-scatter.3.cloned.1.call-done) | copy-start | bytes 589828
Sparse Core Ops, SparseCore 0:
  58.3 24.4 reduce-scatter.2
  388.7 21.4 reduce-scatter.4
Sparse Core Ops, SparseCore 1:
  60.3 107.8 all-gather.3
  169.5 104.8 all-gather.5
  275.8 104.8 all-gather.7
where the time goes:
time: 420 us; the launch traced here: 419 us
  waiting for transfers between devices  323 us (77%)
  blocking collectives  60.2 us (14%)
  between operations  15.2 us (4%)
  matrix products  15.1 us (4%)
  other arithmetic  4.87 us (1%)
    all_gather x1, waiting for transfers between devices, per_device(): lax.all_gather(down_weight, 'sp', axis=1, tiled=True)  106 us
    all_gather x1, waiting for transfers between devices, per_device(): lax.all_gather(up_weight, 'sp', axis=0, tiled=True)  102 us
    all_gather x1, waiting for transfers between devices, per_device(): lax.all_gather(gate_weight, 'sp', axis=0, tiled=True)  68.7 us
    reduce_scatter x1, waiting for transfers between devices, per_device(): lax.psum_scatter(mixed_part.astype(jnp.bfloat16), 'tp', scatter_dimension...  22.8 us
    reduce_scatter x1, waiting for transfers between devices, per_device(): lax.psum_scatter(partial_out.astype(jnp.bfloat16), 'tp', scatter_dimensio...  21.6 us
    all_gather x1, blocking collectives, per_device(): lax.all_gather(key_second, 'sp', axis=0, tiled=True)  16.6 us
    all_gather x1, blocking collectives, per_device(): lax.all_gather(values, 'sp', axis=0, tiled=True)  14.8 us
    all_gather x1, blocking collectives, per_device(): lax.all_gather(key_first, 'sp', axis=0, tiled=True)  14.4 us
  transfers between devices with their start and end apart: 5, of which 5 were waited for; matrix products, arithmetic and copies ran while one was open for 1% of the time, Pallas kernels for 0%

commit v1 on v0

--- a/solution.py
+++ b/solution.py
@@ -1,6 +1,10 @@
+import functools
+
 import jax
 import jax.numpy as jnp
 from jax import lax
+from jax.experimental import pallas as pl
+from jax.experimental.pallas import tpu as pltpu
 from jax.sharding import PartitionSpec as P
 
 D = 2048
@@ -101,9 +105,473 @@
     return (stream + 0.5 * ffn).astype(jnp.bfloat16)
 
 
+def flip(index, bits):
+    bit = 1
+    while bit <= bits:
+        if (bits // bit) % 2:
+            index = index + bit - 2 * bit * ((index // bit) % 2)
+        bit *= 2
+    return index
+
+
+def nt_dot(a, b):
+    return lax.dot_general(a, b, (((1,), (1,)), ((), ())), preferred_element_type=jnp.float32)
+
+
+def dot(a, b):
+    return jnp.dot(a, b, preferred_element_type=jnp.float32)
+
+
+def layer_kernel(
+    sp_count,
+    widths,
+    q_ref,
+    kv_ref,
+    lam_ref,
+    residual_ref,
+    gain_ref,
+    proj_ref,
+    gate_ref,
+    up_ref,
+    down_ref,
+    out_ref,
+    kvb,
+    peak,
+    total,
+    acc,
+    wg,
+    wu,
+    wd,
+    mp,
+    rsb,
+    stream,
+    act,
+    gains,
+    hid,
+    c1,
+    c1r,
+    po,
+    c2,
+    c2r,
+    c3,
+    c3r,
+    kv_ss,
+    kv_rs,
+    w_ss,
+    w_rs,
+    f_ss,
+    f_rs,
+    own_sem,
+    g_ss,
+    g_rs,
+    rs_ss,
+    rs_rs,
+    az_ss,
+    az_rs,
+    ax_ss,
+    ax_rs,
+    ac_ss,
+    ac_rs,
+    c_ss,
+    c_rs,
+):
+    s = lax.axis_index("sp")
+    t = lax.axis_index("tp")
+    y = lax.axis_index("grp")
+    rows, blk = residual_ref.shape
+    cols = wg.shape[2]
+    hidden_all = gate_ref.shape[1]
+    value_size = acc.shape[2]
+    xpeer, cpeer, dpeer = flip(t, 2), flip(t, 1), flip(t, 3)
+    others = range(1, sp_count)
+
+    def remote(src, dst, ssem, rsem, **where):
+        return pltpu.make_async_remote_copy(
+            src_ref=src,
+            dst_ref=dst,
+            send_sem=ssem,
+            recv_sem=rsem,
+            device_id=where,
+            device_id_type=pl.DeviceIdType.MESH,
+        )
+
+    barrier = pltpu.get_barrier_semaphore()
+    for k in others:
+        pl.semaphore_signal(barrier, inc=1, device_id={"sp": flip(s, k)}, device_id_type=pl.DeviceIdType.MESH)
+        pl.semaphore_signal(barrier, inc=1, device_id={"tp": flip(t, k)}, device_id_type=pl.DeviceIdType.MESH)
+    pl.semaphore_signal(barrier, inc=1, device_id={"grp": 1 - y}, device_id_type=pl.DeviceIdType.MESH)
+    pl.semaphore_wait(barrier, 2 * (sp_count - 1) + 1)
+
+    sends = []
+
+    kv_copies = {}
+    for k in others:
+        copy = remote(kv_ref, kvb.at[k], kv_ss.at[k], kv_rs.at[k], sp=flip(s, k))
+        kv_copies[k] = copy
+
+        @pl.when(flip(s, k) > s)
+        def _(copy=copy):
+            copy.start()
+
+    def start_of(index):
+        return pl.multiple_of(jnp.minimum(index * cols, hidden_all - cols), 128)
+
+    half_d = wg.shape[1] // 2
+    half_c = cols // 2
+    d_half = pl.ds(pl.multiple_of(y * half_d, half_d), half_d)
+    c_half = pl.ds(pl.multiple_of(y * half_c, half_c), half_c)
+    w_copies = {}
+    for kind, (src, dst) in enumerate(((gate_ref, wg), (up_ref, wu), (down_ref, wd))):
+        for k in others:
+            begin = start_of(flip(s, k))
+            if kind < 2:
+                piece, place = src.at[d_half, pl.ds(begin, cols)], dst.at[s, d_half]
+            else:
+                piece = src.at[pl.ds(pl.multiple_of(begin + y * half_c, 64), half_c), :]
+                place = dst.at[s, c_half]
+            w_copies[kind, k] = remote(piece, place, w_ss.at[kind, k], w_rs.at[kind, k], sp=flip(s, k))
+    for kinds in ((0, 1), (2,)):
+        for k in others:
+            for kind in kinds:
+                w_copies[kind, k].start()
+                sends.append(w_copies[kind, k])
+    begin = start_of(s)
+    own = [
+        pltpu.make_async_copy(gate_ref.at[:, pl.ds(begin, cols)], wg.at[s], own_sem.at[0]),
+        pltpu.make_async_copy(up_ref.at[:, pl.ds(begin, cols)], wu.at[s], own_sem.at[1]),
+        pltpu.make_async_copy(down_ref.at[pl.ds(begin, cols), :], wd.at[s], own_sem.at[2]),
+    ]
+    for copy in own:
+        copy.start()
+
+    gain_copies = []
+    for k in others:
+        copy = remote(gain_ref, gains.at[t], g_ss.at[k], g_rs.at[k], tp=flip(t, k))
+        copy.start()
+        gain_copies.append(copy)
+        sends.append(copy)
+    gains[t] = gain_ref[...]
+
+    q_at = (0, 2 * widths[0])
+    v_at = 2 * widths[0] + 2 * widths[1]
+    lane = lax.broadcasted_iota(jnp.int32, (1, 2 * widths[0]), 1)
+
+    def block(read, diagonal):
+        for group in range(2):
+            width = widths[group]
+            values = read(v_at + group * value_size, value_size)
+            for m in range(2):
+                if width % 128:
+                    span = (q_at[group], 2 * width)
+                    queries = q_ref[:, span[0] : span[0] + span[1]]
+                    queries = jnp.where(lane // width == m, queries.astype(jnp.float32), 0.0).astype(jnp.bfloat16)
+                else:
+                    span = (q_at[group] + m * width, width)
+                    queries = q_ref[:, span[0] : span[0] + span[1]]
+                scores = nt_dot(queries, read(*span)) * width ** (-0.5)
+                state = 2 * group + m
+                if diagonal:
+                    allowed = lax.broadcasted_iota(jnp.int32, (rows, rows), 1) <= lax.broadcasted_iota(
+                        jnp.int32, (rows, rows), 0
+                    )
+                    scores = jnp.where(allowed, scores, -1e30)
+                    top = jnp.max(scores, axis=1, keepdims=True)
+                    weights = jnp.exp(scores - top)
+                    peak[state] = top
+                    total[state] = jnp.sum(weights, axis=1, keepdims=True)
+                    acc[state] = dot(weights.astype(jnp.bfloat16), values)
+                else:
+                    before = peak[state]
+                    top = jnp.maximum(before, jnp.max(scores, axis=1, keepdims=True))
+                    fade = jnp.exp(before - top)
+                    weights = jnp.exp(scores - top)
+                    peak[state] = top
+                    total[state] = total[state] * fade + jnp.sum(weights, axis=1, keepdims=True)
+                    acc[state] = acc[state] * fade + dot(weights.astype(jnp.bfloat16), values)
+
+    block(lambda at, size: kv_ref[:, at : at + size], True)
+    for k in others:
+
+        @pl.when(flip(s, k) < s)
+        def _(k=k):
+            kv_copies[k].wait_recv()
+            block(lambda at, size: kvb[k, :, at : at + size], False)
+
+    attended = []
+    for group in range(2):
+        first = acc[2 * group] / total[2 * group]
+        second = acc[2 * group + 1] / total[2 * group + 1]
+        differ = first - lam_ref[group, 0] * second
+        scale = lax.rsqrt(jnp.mean(differ * differ, axis=1, keepdims=True) + 1e-06)
+        attended.append((0.8 * differ * scale).astype(jnp.bfloat16))
+
+    def project(owner):
+        columns = pl.ds(pl.multiple_of(owner * blk, blk), blk)
+        return dot(attended[0], proj_ref[:value_size, columns]) + dot(attended[1], proj_ref[value_size:, columns])
+
+    rs_copies = {}
+    for k in (2, 3, 1):
+        mp[k] = project(flip(t, k)).astype(jnp.bfloat16)
+        rs_copies[k] = remote(mp.at[k], rsb.at[k], rs_ss.at[k], rs_rs.at[k], tp=flip(t, k))
+        rs_copies[k].start()
+        sends.append(rs_copies[k])
+    mixed = project(t)
+    for k in (1, 2, 3):
+        rs_copies[k].wait_recv()
+        mixed = mixed + rsb[k].astype(jnp.float32)
+    stream[...] = residual_ref[...].astype(jnp.float32) + mixed
+    act[t, s] = stream[...].astype(jnp.bfloat16)
+
+    az, ax, ac0, ac1 = {}, {}, {}, {}
+    for k in range(sp_count):
+        row = flip(s, k)
+        if k:
+            az[k] = remote(act.at[t, s], act.at[t, s], az_ss.at[k], az_rs.at[k], sp=row)
+        ax[k] = remote(act.at[t, row], act.at[t, row], ax_ss.at[k], ax_rs.at[k], tp=xpeer)
+        ac0[k] = remote(act.at[t, row], act.at[t, row], ac_ss.at[0, k], ac_rs.at[0, k], tp=cpeer)
+        ac1[k] = remote(act.at[xpeer, row], act.at[xpeer, row], ac_ss.at[1, k], ac_rs.at[1, k], tp=cpeer)
+    for k in others:
+        az[k].start()
+
+    def pass_on(k):
+        if k:
+            az[k].wait_recv()
+        ax[k].start()
+        ac0[k].start()
+
+    def pass_inside(k):
+        ax[k].wait_recv()
+        ac1[k].start()
+
+    fw = {}
+
+    def hand_over(kind, k):
+        w_copies[kind, k].wait_recv()
+        buffer = (wg, wu, wd)[kind]
+        piece = buffer.at[flip(s, k), d_half if kind < 2 else c_half]
+        fw[kind, k] = remote(piece, piece, f_ss.at[kind, k], f_rs.at[kind, k], grp=1 - y)
+        fw[kind, k].start()
+        sends.append(fw[kind, k])
+
+    pass_on(0)
+    for k in others:
+        for kind in (0, 1):
+            hand_over(kind, k)
+        pass_on(k)
+        pass_inside(k - 1)
+    for k in others:
+        hand_over(2, k)
+    pass_inside(sp_count - 1)
+
+    for copy in gain_copies:
+        copy.wait_recv()
+    for kind in (0, 1):
+        own[kind].wait()
+        for k in others:
+            fw[kind, k].wait_recv()
+    column = start_of(s) + lax.broadcasted_iota(jnp.int32, (1, cols), 1)
+    mine = column >= s * cols
+
+    def hidden_of(k):
+        row = flip(s, k)
+        ac0[k].wait_recv()
+        ac1[k].wait_recv()
+        squares = jnp.zeros((rows, 1), jnp.float32)
+        for part in range(sp_count):
+            piece = act[part, row].astype(jnp.float32)
+            squares = squares + jnp.sum(piece * piece, axis=1, keepdims=True)
+        scale = lax.rsqrt(squares / (sp_count * blk) + 1e-06)
+        gate = jnp.zeros((rows, cols), jnp.float32)
+        up = jnp.zeros((rows, cols), jnp.float32)
+        for part in range(sp_count):
+            gain = gains[part, 0:1, :].astype(jnp.float32)
+            normed = (act[part, row].astype(jnp.float32) * scale * gain).astype(jnp.bfloat16)
+            gate = gate + dot(normed, wg[part])
+            up = up + dot(normed, wu[part])
+        hidden = gate / (1.0 + jnp.exp(-gate)) * up
+        hid[k] = jnp.where(mine, hidden, 0.0).astype(jnp.bfloat16)
+
+    r1, r2, r3 = {}, {}, {}
+    for k in range(sp_count):
+        r1[k] = remote(c1.at[k], c1r.at[k], c_ss.at[0, k], c_rs.at[0, k], tp=cpeer)
+        r2[k] = remote(c2.at[k], c2r.at[k], c_ss.at[1, k], c_rs.at[1, k], tp=xpeer)
+        if k:
+            r3[k] = remote(c3.at[k], c3r.at[k], c_ss.at[2, k], c_rs.at[2, k], sp=flip(s, k))
+
+    def down_of(k):
+        hidden = hid[k]
+        c1[k, 0] = dot(hidden, wd[cpeer]).astype(jnp.bfloat16)
+        c1[k, 1] = dot(hidden, wd[dpeer]).astype(jnp.bfloat16)
+        r1[k].start()
+        po[k, 1] = dot(hidden, wd[xpeer])
+        po[k, 0] = dot(hidden, wd[t])
+
+    def across(k):
+        r1[k].wait_recv()
+        c2[k] = (po[k, 1] + c1r[k, 1].astype(jnp.float32)).astype(jnp.bfloat16)
+        r2[k].start()
+
+    def along(k):
+        r2[k].wait_recv()
+        result = po[k, 0] + c1r[k, 0].astype(jnp.float32) + c2r[k].astype(jnp.float32)
+        if k:
+            c3[k] = result.astype(jnp.bfloat16)
+            r3[k].start()
+        else:
+            po[0, 0] = result
+
+    order = (3, 2, 1, 0)
+    first = True
+    for at, k in enumerate(order):
+        hidden_of(k)
+        if first:
+            own[2].wait()
+            for j in others:
+                fw[2, j].wait_recv()
+            first = False
+        down_of(k)
+        if at >= 1:
+            across(order[at - 1])
+        if at >= 2:
+            along(order[at - 2])
+    across(order[-1])
+    along(order[-2])
+    along(order[-1])
+
+    ffn = po[0, 0]
+    for k in order[:-1]:
+        r3[k].wait_recv()
+        ffn = ffn + c3r[k].astype(jnp.float32)
+    out_ref[...] = (stream[...] + 0.5 * ffn).astype(jnp.bfloat16)
+
+    for k in others:
+
+        @pl.when(flip(s, k) > s)
+        def _(k=k):
+            kv_copies[k].wait_send()
+
+    for copies in (az, ax, ac0, ac1, r1, r2, r3):
+        sends.extend(copies.values())
+    for copy in sends:
+        copy.wait_send()
+
+
+def fits(axes, query_first, values, lambdas, residual, gate_weight):
+    sp, tp = axes["sp"], axes["tp"]
+    rows, blk = residual.shape
+    depth, hidden_all = gate_weight.shape
+    if axes["grp"] != 2 or sp != tp or tp != 4 or lambdas.shape[1] != 1:
+        return False
+    if depth != blk or blk % 128 or hidden_all % 128 or rows % 16:
+        return False
+    if (2 * query_first.shape[1]) % 256 or values.shape[2] % 128:
+        return False
+    cols = -(-hidden_all // (128 * sp)) * 128
+    if cols * sp - hidden_all >= cols or cols > hidden_all:
+        return False
+    need = 6 * sp * blk * cols + rows * blk * 2 * 20 * sp
+    return need < 40 * 1024 * 1024
+
+
+def one_device(
+    axes,
+    query_first,
+    key_first,
+    query_second,
+    key_second,
+    values,
+    lambdas,
+    residual,
+    norm_gain,
+    out_weight,
+    gate_weight,
+    up_weight,
+    down_weight,
+):
+    if not fits(axes, query_first, values, lambdas, residual, gate_weight):
+        return per_device(
+            query_first,
+            key_first,
+            query_second,
+            key_second,
+            values,
+            lambdas,
+            residual,
+            norm_gain,
+            out_weight,
+            gate_weight,
+            up_weight,
+            down_weight,
+        )
+    n = axes["sp"]
+    rows, blk = residual.shape
+    hidden_all = gate_weight.shape[1]
+    cols = -(-hidden_all // (128 * n)) * 128
+    value_size = values.shape[2]
+    widths = (query_first.shape[1] // 2, query_second.shape[1] // 2)
+    queries = jnp.concatenate([query_first, query_second], axis=1)
+    kv = jnp.concatenate([key_first, key_second, values[:, 0], values[:, 1]], axis=1)
+    gain = jnp.broadcast_to(norm_gain[None, :], (16, blk))
+    projection = out_weight.reshape(2 * value_size, out_weight.shape[2])
+    bf16, f32 = jnp.bfloat16, jnp.float32
+    vmem = pl.BlockSpec(memory_space=pltpu.VMEM)
+    smem = pl.BlockSpec(memory_space=pltpu.SMEM)
+    hbm = pl.BlockSpec(memory_space=pl.ANY)
+    dma = pltpu.SemaphoreType.DMA
+    return pl.pallas_call(
+        functools.partial(layer_kernel, n, widths),
+        out_shape=jax.ShapeDtypeStruct((rows, blk), bf16),
+        in_specs=[vmem, vmem, smem, vmem, vmem, vmem, hbm, hbm, hbm],
+        out_specs=vmem,
+        scratch_shapes=[
+            pltpu.VMEM((n,) + kv.shape, bf16),
+            pltpu.VMEM((4, rows, 1), f32),
+            pltpu.VMEM((4, rows, 1), f32),
+            pltpu.VMEM((4, rows, value_size), f32),
+            pltpu.VMEM((n, blk, cols), bf16),
+            pltpu.VMEM((n, blk, cols), bf16),
+            pltpu.VMEM((n, cols, blk), bf16),
+            pltpu.VMEM((n, rows, blk), bf16),
+            pltpu.VMEM((n, rows, blk), bf16),
+            pltpu.VMEM((rows, blk), f32),
+            pltpu.VMEM((n, n, rows, blk), bf16),
+            pltpu.VMEM((n, 16, blk), bf16),
+            pltpu.VMEM((n, rows, cols), bf16),
+            pltpu.VMEM((n, 2, rows, blk), bf16),
+            pltpu.VMEM((n, 2, rows, blk), bf16),
+            pltpu.VMEM((n, 2, rows, blk), f32),
+            pltpu.VMEM((n, rows, blk), bf16),
+            pltpu.VMEM((n, rows, blk), bf16),
+            pltpu.VMEM((n, rows, blk), bf16),
+            pltpu.VMEM((n, rows, blk), bf16),
+            dma((n,)),
+            dma((n,)),
+            dma((3, n)),
+            dma((3, n)),
+            dma((3, n)),
+            dma((3, n)),
+            dma((3,)),
+            dma((n,)),
+            dma((n,)),
+            dma((n,)),
+            dma((n,)),
+            dma((n,)),
+            dma((n,)),
+            dma((n,)),
+            dma((n,)),
+            dma((2, n)),
+            dma((2, n)),
+            dma((3, n)),
+            dma((3, n)),
+        ],
+        compiler_params=pltpu.CompilerParams(
+            collective_id=0, has_side_effects=True, vmem_limit_bytes=60 * 1024 * 1024
+        ),
+    )(queries, kv, lambdas, residual, gain, projection, gate_weight, up_weight, down_weight)
+
 def solution(mesh):
     return jax.shard_map(
-        per_device,
+        functools.partial(one_device, dict(mesh.shape)),
         mesh=mesh,
         in_specs=(
             P(("grp", "sp"), "tp"),

time: 420 us -> 149 us (0.35)
  waiting for transfers between devices: 323 us -> 0 us
  Pallas kernels: 0 us -> 140 us
  blocking collectives: 60.2 us -> 0 us
  between operations: 15.2 us -> 0.02 us
  matrix products: 15.1 us -> 0 us
  local copies, waits for them, and re-layouts: 0.68 us -> 5.35 us
    all_gather x3 -> x0, waiting for transfers between devices: 277 us -> none  [the longest x1 106 us: per_device(): lax.all_gather(down_weight, 'sp', axis=1, tiled=True)]
    pallas_call x0 -> x1, Pallas kernels: none -> 140 us  [one_device(): pl.pallas_call(functools.partial(layer_kernel, n, widths), out_shape=jax....]
    all_gather x4 -> x0, blocking collectives: 54.1 us -> none  [the longest x1 16.6 us: per_device(): lax.all_gather(key_second, 'sp', axis=0, tiled=True)]
    reduce_scatter x2 -> x0, waiting for transfers between devices: 44.4 us -> none  [the longest x1 22.8 us: per_device(): lax.psum_scatter(mixed_part.astype(jnp.bfloat16), 'tp', scatter_dimension...]
    dot_general x7 -> x0, matrix products: 15.1 us -> none  [the longest x1 7.87 us: per_device(): jnp.dot(hidden, lax.all_gather(down_weight, 'sp', axis=1, tiled=True), pr...]
    psum x1 -> x0, blocking collectives: 6.06 us -> none  [per_device(): squares = lax.psum(jnp.sum(stream * stream, axis=1), 'tp')]
  transfers between devices with their start and end apart: 5 -> 0, of which waited for: 5 -> 0; matrix products, arithmetic and copies ran while one was open for 1% -> 0% of each run, Pallas kernels for 0% -> 0%
where the time goes in v1:
time: 149 us
  Pallas kernels  140 us (94%)
  local copies, waits for them, and re-layouts  5.35 us (4%)
  other arithmetic  3.19 us (2%)
    pallas_call x1, Pallas kernels, one_device(): pl.pallas_call(functools.partial(layer_kernel, n, widths), out_shape=jax....  140 us

profile of v1, /device:TPU:0, one launch (start us, length us, event | category | flops | bytes accessed | tf_op | source)
XLA Modules:
  0.0 148.6 jit_solution(17306056933699063228)
XLA Ops:
  0.0 1.3 copy.15.lam_ref
  1.3 1.3 broadcast_in_dim.2.gain_ref
  2.6 1.6 %pad_maximum_fusion.1.q_ref = bf16[192,384]{1,0:T(8,128)(2,1)} fusion(bf16[192,256]{1,0:T(8,128)(2,1)} %param.14, bf16[192,128]{1,0:T(8,128)(2,1)} %param.12), kind=kLoop, calls=%fused_computation.1 | loop fusion | flops 294912 | bytes 294912 | tf_op jit(solution)/shard_map/concatenate | solution.py:512
  4.2 1.1 fusion
  5.3 1.6 %pad_maximum_fusion.kv_ref = bf16[192,640]{1,0:T(8,128)(2,1)} fusion(bf16[192,128]{1,0:T(8,128)(2,1)S(1)} %get-tuple-element.7, bf16[192,128]{1,0:T(8,128)(2,1)S(1)} %get-tuple-element.8, bf16[192,256]{1,0:T(8,128)(2,1)} %param.15, bf16[192,128]{1,0:T(8,128)(2,1)} %param.13), kind=kLoop, calls=%fused_computation | loop fusion | flops 983040 | bytes 491520 | tf_op jit(solution)/shard_map/concatenate | solution.py:513
  6.9 140.1 %shard_map.118 = bf16[192,512]{1,0:T(8,128)(2,1)} custom-call(bf16[192,384]{1,0:T(8,128)(2,1)} %pad_maximum_fusion.1.q_ref, bf16[192,640]{1,0:T(8,128)(2,1)} %pad_maximum_fusion.kv_ref, f32[2,1]{1,0:T(2,128)} %copy.15.lam_ref, bf16[192,512]{1,0:T(8,128)(2,1)} %residual_ref.1, bf16[16,512]{1,0:T(8,128)(2,1)} %broadcast_in_dim.2.gain_ref, ...), custom_call_target="tpu_custom_call" | custom-call | tf_op jit(solution)/shard_map/pallas_call | solution.py:521
  147.0 1.6 %copy.21 = bf16[192,512]{1,0:T(8,128)(2,1)} copy(bf16[192,512]{1,0:T(8,128)(2,1)} %shard_map.118) | data formatting | bytes 393216
  (1 shorter events, 0.0 us)

commit v2 on v1

--- a/solution.py
+++ b/solution.py
@@ -125,17 +125,23 @@
 def layer_kernel(
     sp_count,
     widths,
-    q_ref,
-    kv_ref,
+    q1_ref,
+    q2_ref,
+    k1_ref,
+    k2_ref,
+    v_ref,
     lam_ref,
     residual_ref,
     gain_ref,
-    proj_ref,
+    proj_hbm,
     gate_ref,
     up_ref,
     down_ref,
     out_ref,
-    kvb,
+    k1b,
+    k2b,
+    vb,
+    proj_ref,
     peak,
     total,
     acc,
@@ -206,69 +212,100 @@
 
     kv_copies = {}
     for k in others:
-        copy = remote(kv_ref, kvb.at[k], kv_ss.at[k], kv_rs.at[k], sp=flip(s, k))
-        kv_copies[k] = copy
+        kv_copies[k] = [
+            remote(src, dst.at[k], kv_ss.at[i, k], kv_rs.at[i, k], sp=flip(s, k))
+            for i, (src, dst) in enumerate(((k1_ref, k1b), (k2_ref, k2b), (v_ref, vb)))
+        ]
 
         @pl.when(flip(s, k) > s)
-        def _(copy=copy):
-            copy.start()
-
-    def start_of(index):
-        return pl.multiple_of(jnp.minimum(index * cols, hidden_all - cols), 128)
+        def _(k=k):
+            for copy in kv_copies[k]:
+                copy.start()
 
     half_d = wg.shape[1] // 2
     half_c = cols // 2
+    extra = sp_count * cols - hidden_all
+    half_last = (cols - extra) // 2
     d_half = pl.ds(pl.multiple_of(y * half_d, half_d), half_d)
-    c_half = pl.ds(pl.multiple_of(y * half_c, half_c), half_c)
-    w_copies = {}
-    for kind, (src, dst) in enumerate(((gate_ref, wg), (up_ref, wu), (down_ref, wd))):
+    last = sp_count - 1
+
+    def w_copy(kind, k, source, target, short):
+        src, dst = ((gate_ref, wg), (up_ref, wu), (down_ref, wd))[kind]
+        begin = hidden_all - cols + extra if short else pl.multiple_of(target * cols, 128)
+        skip, size = (extra, cols - extra) if short else (0, cols)
+        if kind < 2:
+            piece = src.at[d_half, pl.ds(begin, size)]
+            place = dst.at[source, d_half, pl.ds(skip, size)]
+        else:
+            part = y * (size // 2)
+            piece = src.at[pl.ds(pl.multiple_of(begin + part, 64), size // 2), :]
+            place = dst.at[source, pl.ds(pl.multiple_of(skip + part, 64), size // 2)]
+        return remote(piece, place, w_ss.at[kind, k], w_rs.at[kind, k], sp=flip(s, k)), place
+
+    def f_copy(kind, k, short):
+        _, place = w_copy(kind, k, flip(s, k), s, short)
+        return remote(place, place, f_ss.at[kind, k], f_rs.at[kind, k], grp=1 - y)
+
+    def either(test, action):
+        pl.when(test)(lambda: action(True))
+        pl.when(jnp.logical_not(test))(lambda: action(False))
+
+    def send_weights(kinds):
         for k in others:
-            begin = start_of(flip(s, k))
-            if kind < 2:
-                piece, place = src.at[d_half, pl.ds(begin, cols)], dst.at[s, d_half]
-            else:
-                piece = src.at[pl.ds(pl.multiple_of(begin + y * half_c, 64), half_c), :]
-                place = dst.at[s, c_half]
-            w_copies[kind, k] = remote(piece, place, w_ss.at[kind, k], w_rs.at[kind, k], sp=flip(s, k))
-    for kinds in ((0, 1), (2,)):
-        for k in others:
-            for kind in kinds:
-                w_copies[kind, k].start()
-                sends.append(w_copies[kind, k])
-    begin = start_of(s)
-    own = [
-        pltpu.make_async_copy(gate_ref.at[:, pl.ds(begin, cols)], wg.at[s], own_sem.at[0]),
-        pltpu.make_async_copy(up_ref.at[:, pl.ds(begin, cols)], wu.at[s], own_sem.at[1]),
-        pltpu.make_async_copy(down_ref.at[pl.ds(begin, cols), :], wd.at[s], own_sem.at[2]),
-    ]
-    for copy in own:
-        copy.start()
-
+
+            def go(short, k=k):
+                for kind in kinds:
+                    w_copy(kind, k, s, flip(s, k), short)[0].start()
+
+            either(flip(s, k) == last, go)
+
+    @pl.when(s == last)
+    def _():
+        wg[:, :, :extra] = jnp.zeros((sp_count, wg.shape[1], extra), jnp.bfloat16)
+        wu[:, :, :extra] = jnp.zeros((sp_count, wg.shape[1], extra), jnp.bfloat16)
+        wd[:, :extra, :] = jnp.zeros((sp_count, extra, blk), jnp.bfloat16)
+
+    send_weights((0, 1))
+    proj_copy = pltpu.make_async_copy(proj_hbm, proj_ref, own_sem.at[3])
+    proj_copy.start()
+    def own_copy(kind, short):
+        src, dst = ((gate_ref, wg), (up_ref, wu), (down_ref, wd))[kind]
+        begin = hidden_all - cols + extra if short else pl.multiple_of(s * cols, 128)
+        skip, size = (extra, cols - extra) if short else (0, cols)
+        if kind < 2:
+            return pltpu.make_async_copy(src.at[:, pl.ds(begin, size)], dst.at[s, :, pl.ds(skip, size)], own_sem.at[kind])
+        return pltpu.make_async_copy(src.at[pl.ds(begin, size), :], dst.at[s, pl.ds(skip, size)], own_sem.at[kind])
+
+    def start_own(short):
+        for kind in range(3):
+            own_copy(kind, short).start()
+
+    either(s == last, start_own)
+
+    gains[t] = jnp.broadcast_to(gain_ref[...].reshape(1, blk), gains.shape[1:])
     gain_copies = []
     for k in others:
-        copy = remote(gain_ref, gains.at[t], g_ss.at[k], g_rs.at[k], tp=flip(t, k))
+        copy = remote(gains.at[t], gains.at[t], g_ss.at[k], g_rs.at[k], tp=flip(t, k))
         copy.start()
         gain_copies.append(copy)
         sends.append(copy)
-    gains[t] = gain_ref[...]
-
-    q_at = (0, 2 * widths[0])
-    v_at = 2 * widths[0] + 2 * widths[1]
+
+    q_refs = (q1_ref, q2_ref)
     lane = lax.broadcasted_iota(jnp.int32, (1, 2 * widths[0]), 1)
 
-    def block(read, diagonal):
+    def block(keys, v, diagonal):
         for group in range(2):
             width = widths[group]
-            values = read(v_at + group * value_size, value_size)
+            values = v[:, group, :]
             for m in range(2):
                 if width % 128:
-                    span = (q_at[group], 2 * width)
-                    queries = q_ref[:, span[0] : span[0] + span[1]]
+                    span = slice(0, 2 * width)
+                    queries = q_refs[group][:, span]
                     queries = jnp.where(lane // width == m, queries.astype(jnp.float32), 0.0).astype(jnp.bfloat16)
                 else:
-                    span = (q_at[group] + m * width, width)
-                    queries = q_ref[:, span[0] : span[0] + span[1]]
-                scores = nt_dot(queries, read(*span)) * width ** (-0.5)
+                    span = slice(m * width, (m + 1) * width)
+                    queries = q_refs[group][:, span]
+                scores = nt_dot(queries, keys[group][:, span]) * width ** (-0.5)
                 state = 2 * group + m
                 if diagonal:
                     allowed = lax.broadcasted_iota(jnp.int32, (rows, rows), 1) <= lax.broadcasted_iota(
@@ -289,25 +326,27 @@
                     total[state] = total[state] * fade + jnp.sum(weights, axis=1, keepdims=True)
                     acc[state] = acc[state] * fade + dot(weights.astype(jnp.bfloat16), values)
 
-    block(lambda at, size: kv_ref[:, at : at + size], True)
+    block((k1_ref, k2_ref), v_ref, True)
     for k in others:
 
         @pl.when(flip(s, k) < s)
         def _(k=k):
-            kv_copies[k].wait_recv()
-            block(lambda at, size: kvb[k, :, at : at + size], False)
-
+            for copy in kv_copies[k]:
+                copy.wait_recv()
+            block((k1b.at[k], k2b.at[k]), vb.at[k], False)
+
+    proj_copy.wait()
     attended = []
     for group in range(2):
         first = acc[2 * group] / total[2 * group]
         second = acc[2 * group + 1] / total[2 * group + 1]
-        differ = first - lam_ref[group, 0] * second
+        differ = first - lam_ref[0, group] * second
         scale = lax.rsqrt(jnp.mean(differ * differ, axis=1, keepdims=True) + 1e-06)
         attended.append((0.8 * differ * scale).astype(jnp.bfloat16))
 
     def project(owner):
         columns = pl.ds(pl.multiple_of(owner * blk, blk), blk)
-        return dot(attended[0], proj_ref[:value_size, columns]) + dot(attended[1], proj_ref[value_size:, columns])
+        return dot(attended[0], proj_ref[0, :, columns]) + dot(attended[1], proj_ref[1, :, columns])
 
     rs_copies = {}
     for k in (2, 3, 1):
@@ -332,6 +371,7 @@
         ac1[k] = remote(act.at[xpeer, row], act.at[xpeer, row], ac_ss.at[1, k], ac_rs.at[1, k], tp=cpeer)
     for k in others:
         az[k].start()
+    send_weights((2,))
 
     def pass_on(k):
         if k:
@@ -343,33 +383,34 @@
         ax[k].wait_recv()
         ac1[k].start()
 
-    fw = {}
-
-    def hand_over(kind, k):
-        w_copies[kind, k].wait_recv()
-        buffer = (wg, wu, wd)[kind]
-        piece = buffer.at[flip(s, k), d_half if kind < 2 else c_half]
-        fw[kind, k] = remote(piece, piece, f_ss.at[kind, k], f_rs.at[kind, k], grp=1 - y)
-        fw[kind, k].start()
-        sends.append(fw[kind, k])
+    def hand_over(kinds, k):
+        def go(short):
+            for kind in kinds:
+                w_copy(kind, k, flip(s, k), s, short)[0].wait_recv()
+                f_copy(kind, k, short).start()
+
+        either(s == last, go)
+
+    def await_weights(kinds):
+        def go(short):
+            for kind in kinds:
+                own_copy(kind, short).wait()
+                for k in others:
+                    f_copy(kind, k, short).wait_recv()
+
+        either(s == last, go)
 
     pass_on(0)
     for k in others:
-        for kind in (0, 1):
-            hand_over(kind, k)
+        hand_over((0, 1), k)
         pass_on(k)
         pass_inside(k - 1)
-    for k in others:
-        hand_over(2, k)
     pass_inside(sp_count - 1)
 
     for copy in gain_copies:
         copy.wait_recv()
-    for kind in (0, 1):
-        own[kind].wait()
-        for k in others:
-            fw[kind, k].wait_recv()
-    column = start_of(s) + lax.broadcasted_iota(jnp.int32, (1, cols), 1)
+    await_weights((0, 1))
+    column = jnp.minimum(s * cols, hidden_all - cols) + lax.broadcasted_iota(jnp.int32, (1, cols), 1)
     mine = column >= s * cols
 
     def hidden_of(k):
@@ -425,9 +466,9 @@
     for at, k in enumerate(order):
         hidden_of(k)
         if first:
-            own[2].wait()
             for j in others:
-                fw[2, j].wait_recv()
+                hand_over((2,), j)
+            await_weights((2,))
             first = False
         down_of(k)
         if at >= 1:
@@ -448,8 +489,26 @@
 
         @pl.when(flip(s, k) > s)
         def _(k=k):
-            kv_copies[k].wait_send()
-
+            for copy in kv_copies[k]:
+                copy.wait_send()
+
+    def finish():
+        for k in others:
+
+            def go(short, k=k):
+                for kind in range(3):
+                    w_copy(kind, k, s, flip(s, k), short)[0].wait_send()
+
+            either(flip(s, k) == last, go)
+
+        def gone(short):
+            for k in others:
+                for kind in range(3):
+                    f_copy(kind, k, short).wait_send()
+
+        either(s == last, gone)
+
+    finish()
     for copies in (az, ax, ac0, ac1, r1, r2, r3):
         sends.extend(copies.values())
     for copy in sends:
@@ -468,6 +527,8 @@
         return False
     cols = -(-hidden_all // (128 * sp)) * 128
     if cols * sp - hidden_all >= cols or cols > hidden_all:
+        return False
+    if (cols * sp - hidden_all) % 128 or blk % 32:
         return False
     need = 6 * sp * blk * cols + rows * blk * 2 * 20 * sp
     return need < 40 * 1024 * 1024
@@ -509,10 +570,6 @@
     cols = -(-hidden_all // (128 * n)) * 128
     value_size = values.shape[2]
     widths = (query_first.shape[1] // 2, query_second.shape[1] // 2)
-    queries = jnp.concatenate([query_first, query_second], axis=1)
-    kv = jnp.concatenate([key_first, key_second, values[:, 0], values[:, 1]], axis=1)
-    gain = jnp.broadcast_to(norm_gain[None, :], (16, blk))
-    projection = out_weight.reshape(2 * value_size, out_weight.shape[2])
     bf16, f32 = jnp.bfloat16, jnp.float32
     vmem = pl.BlockSpec(memory_space=pltpu.VMEM)
     smem = pl.BlockSpec(memory_space=pltpu.SMEM)
@@ -521,10 +578,13 @@
     return pl.pallas_call(
         functools.partial(layer_kernel, n, widths),
         out_shape=jax.ShapeDtypeStruct((rows, blk), bf16),
-        in_specs=[vmem, vmem, smem, vmem, vmem, vmem, hbm, hbm, hbm],
+        in_specs=[vmem] * 5 + [smem, vmem, vmem] + [hbm] * 4,
         out_specs=vmem,
         scratch_shapes=[
-            pltpu.VMEM((n,) + kv.shape, bf16),
+            pltpu.VMEM((n,) + key_first.shape, bf16),
+            pltpu.VMEM((n,) + key_second.shape, bf16),
+            pltpu.VMEM((n,) + values.shape, bf16),
+            pltpu.VMEM(out_weight.shape, bf16),
             pltpu.VMEM((4, rows, 1), f32),
             pltpu.VMEM((4, rows, 1), f32),
             pltpu.VMEM((4, rows, value_size), f32),
@@ -544,13 +604,13 @@
             pltpu.VMEM((n, rows, blk), bf16),
             pltpu.VMEM((n, rows, blk), bf16),
             pltpu.VMEM((n, rows, blk), bf16),
-            dma((n,)),
-            dma((n,)),
-            dma((3, n)),
-            dma((3, n)),
-            dma((3, n)),
-            dma((3, n)),
-            dma((3,)),
+            dma((3, n)),
+            dma((3, n)),
+            dma((3, n)),
+            dma((3, n)),
+            dma((3, n)),
+            dma((3, n)),
+            dma((4,)),
             dma((n,)),
             dma((n,)),
             dma((n,)),
@@ -567,7 +627,20 @@
         compiler_params=pltpu.CompilerParams(
             collective_id=0, has_side_effects=True, vmem_limit_bytes=60 * 1024 * 1024
         ),
-    )(queries, kv, lambdas, residual, gain, projection, gate_weight, up_weight, down_weight)
+    )(
+        query_first,
+        query_second,
+        key_first,
+        key_second,
+        values,
+        lambdas.T,
+        residual,
+        norm_gain,
+        out_weight,
+        gate_weight,
+        up_weight,
+        down_weight,
+    )
 
 def solution(mesh):
     return jax.shard_map(

time: 149 us -> 131 us (0.88)
  Pallas kernels: 140 us -> 129 us
  local copies, waits for them, and re-layouts: 5.35 us -> 1.62 us
  other arithmetic: 3.19 us -> 0 us
    pallas_call x1, Pallas kernels: 140 us -> 129 us  [one_device(): pl.pallas_call(functools.partial(layer_kernel, n, widths), out_shape=jax....]
    concatenate x2 -> x0, other arithmetic: 3.19 us -> none  [the longest x1 1.62 us: one_device(): jnp.concatenate([key_first, key_second, values[:, 0], values[:, 1]], axis=1)]
where the time goes in v2:
time: 131 us
  Pallas kernels  129 us (98%)
  local copies, waits for them, and re-layouts  1.62 us (1%)
    pallas_call x1, Pallas kernels, one_device(): pl.pallas_call(functools.partial(layer_kernel, n, widths), out_shape=jax....  129 us

profile of v2, /device:TPU:0, one launch (start us, length us, event | category | flops | bytes accessed | tf_op | source)
XLA Modules:
  0.0 130.6 jit_solution(5689472765224211328)
XLA Ops:
  0.0 129.0 %shard_map.118 = bf16[192,512]{1,0:T(8,128)(2,1)} custom-call(bf16[192,128]{1,0:T(8,128)(2,1)} %q1_ref.1, bf16[192,256]{1,0:T(8,128)(2,1)} %q2_ref.1, bf16[192,128]{1,0:T(8,128)(2,1)} %k1_ref.1, bf16[192,256]{1,0:T(8,128)(2,1)} %k2_ref.1, bf16[192,2,128]{2,1,0:T(2,128)(2,1)} %v_ref.1, f32[1,2]{1,0:T(1,128)} %bitcast.1, bf16[192,512]{1,0:T(8,128)(2,1)} %residual_ref.1, ...), custom_call_target="tpu_custom_call" | custom-call | tf_op jit(solution)/shard_map/pallas_call | solution.py:578
  129.0 1.6 %copy.14 = bf16[192,512]{1,0:T(8,128)(2,1)} copy(bf16[192,512]{1,0:T(8,128)(2,1)} %shard_map.118) | data formatting | bytes 393216

commit v3 on v2

--- a/solution.py
+++ b/solution.py
@@ -210,17 +210,25 @@
 
     sends = []
 
-    kv_copies = {}
-    for k in others:
-        kv_copies[k] = [
-            remote(src, dst.at[k], kv_ss.at[i, k], kv_rs.at[i, k], sp=flip(s, k))
-            for i, (src, dst) in enumerate(((k1_ref, k1b), (k2_ref, k2b), (v_ref, vb)))
+    right, left = lax.rem(s + 1, sp_count), lax.rem(s + sp_count - 1, sp_count)
+    has_right, has_left = s + 1 < sp_count, s > 0
+
+    def kv_copy(back):
+        pairs = ((k1_ref, k1b), (k2_ref, k2b), (v_ref, vb))
+        return [
+            remote(dst.at[back] if back else src, dst.at[back + 1], kv_ss.at[i, back], kv_rs.at[i, back + 1], sp=right)
+            for i, (src, dst) in enumerate(pairs)
         ]
 
-        @pl.when(flip(s, k) > s)
-        def _(k=k):
-            for copy in kv_copies[k]:
+    kv_copies = {back: kv_copy(back) for back in range(sp_count - 1)}
+
+    def kv_send(back):
+        @pl.when(jnp.logical_and(has_right, s >= back))
+        def _():
+            for copy in kv_copies[back]:
                 copy.start()
+
+    kv_send(0)
 
     half_d = wg.shape[1] // 2
     half_c = cols // 2
@@ -250,14 +258,19 @@
         pl.when(test)(lambda: action(True))
         pl.when(jnp.logical_not(test))(lambda: action(False))
 
-    def send_weights(kinds):
+    def send_weights(kinds, rightward):
         for k in others:
 
             def go(short, k=k):
                 for kind in kinds:
                     w_copy(kind, k, s, flip(s, k), short)[0].start()
 
-            either(flip(s, k) == last, go)
+            target = flip(s, k)
+            if rightward:
+                pl.when(target == last)(functools.partial(go, True))
+                pl.when(jnp.logical_and(target > s, target != last))(functools.partial(go, False))
+            else:
+                pl.when(target < s)(functools.partial(go, False))
 
     @pl.when(s == last)
     def _():
@@ -265,7 +278,7 @@
         wu[:, :, :extra] = jnp.zeros((sp_count, wg.shape[1], extra), jnp.bfloat16)
         wd[:, :extra, :] = jnp.zeros((sp_count, extra, blk), jnp.bfloat16)
 
-    send_weights((0, 1))
+    send_weights((0, 1), False)
     proj_copy = pltpu.make_async_copy(proj_hbm, proj_ref, own_sem.at[3])
     proj_copy.start()
     def own_copy(kind, short):
@@ -327,13 +340,21 @@
                     acc[state] = acc[state] * fade + dot(weights.astype(jnp.bfloat16), values)
 
     block((k1_ref, k2_ref), v_ref, True)
-    for k in others:
-
-        @pl.when(flip(s, k) < s)
-        def _(k=k):
-            for copy in kv_copies[k]:
+    for back in others:
+
+        @pl.when(s >= back)
+        def _(back=back):
+            for copy in kv_copies[back - 1]:
                 copy.wait_recv()
-            block((k1b.at[k], k2b.at[k]), vb.at[k], False)
+
+        if back in kv_copies:
+            kv_send(back)
+    send_weights((0, 1), True)
+    for back in others:
+
+        @pl.when(s >= back)
+        def _(back=back):
+            block((k1b.at[back], k2b.at[back]), vb.at[back], False)
 
     proj_copy.wait()
     attended = []
@@ -361,21 +382,35 @@
     stream[...] = residual_ref[...].astype(jnp.float32) + mixed
     act[t, s] = stream[...].astype(jnp.bfloat16)
 
-    az, ax, ac0, ac1 = {}, {}, {}, {}
+    ax, ac0, ac1 = {}, {}, {}
     for k in range(sp_count):
         row = flip(s, k)
-        if k:
-            az[k] = remote(act.at[t, s], act.at[t, s], az_ss.at[k], az_rs.at[k], sp=row)
         ax[k] = remote(act.at[t, row], act.at[t, row], ax_ss.at[k], ax_rs.at[k], tp=xpeer)
         ac0[k] = remote(act.at[t, row], act.at[t, row], ac_ss.at[0, k], ac_rs.at[0, k], tp=cpeer)
         ac1[k] = remote(act.at[xpeer, row], act.at[xpeer, row], ac_ss.at[1, k], ac_rs.at[1, k], tp=cpeer)
-    for k in others:
-        az[k].start()
-    send_weights((2,))
+
+    def along_line(k, action):
+        row = flip(s, k)
+        piece = act.at[t, row]
+
+        @pl.when(jnp.logical_and(has_right, row <= s))
+        def _():
+            action(remote(piece, piece, az_ss.at[0, row], az_rs.at[row], sp=right))
+
+        @pl.when(jnp.logical_and(has_left, row >= s))
+        def _():
+            action(remote(piece, piece, az_ss.at[1, row], az_rs.at[row], sp=left))
+
+    along_line(0, lambda copy: copy.start())
+    send_weights((2,), True)
+    send_weights((2,), False)
 
     def pass_on(k):
         if k:
-            az[k].wait_recv()
+            row = flip(s, k)
+            piece = act.at[t, row]
+            remote(piece, piece, az_ss.at[0, row], az_rs.at[row], sp=right).wait_recv()
+            along_line(k, lambda copy: copy.start())
         ax[k].start()
         ac0[k].start()
 
@@ -400,12 +435,13 @@
 
         either(s == last, go)
 
+    turns = (0, 1, 3, 2)
     pass_on(0)
-    for k in others:
-        hand_over((0, 1), k)
+    for at, k in enumerate(turns[1:]):
+        hand_over((0, 1), at + 1)
         pass_on(k)
-        pass_inside(k - 1)
-    pass_inside(sp_count - 1)
+        pass_inside(turns[at])
+    pass_inside(turns[-1])
 
     for copy in gain_copies:
         copy.wait_recv()
@@ -461,15 +497,13 @@
         else:
             po[0, 0] = result
 
+    for at, k in enumerate(turns):
+        hidden_of(k)
+        if at + 1 < sp_count:
+            hand_over((2,), at + 1)
+    await_weights((2,))
     order = (3, 2, 1, 0)
-    first = True
     for at, k in enumerate(order):
-        hidden_of(k)
-        if first:
-            for j in others:
-                hand_over((2,), j)
-            await_weights((2,))
-            first = False
         down_of(k)
         if at >= 1:
             across(order[at - 1])
@@ -485,11 +519,11 @@
         ffn = ffn + c3r[k].astype(jnp.float32)
     out_ref[...] = (stream[...] + 0.5 * ffn).astype(jnp.bfloat16)
 
-    for k in others:
-
-        @pl.when(flip(s, k) > s)
-        def _(k=k):
-            for copy in kv_copies[k]:
+    for back in kv_copies:
+
+        @pl.when(jnp.logical_and(has_right, s >= back))
+        def _(back=back):
+            for copy in kv_copies[back]:
                 copy.wait_send()
 
     def finish():
@@ -509,7 +543,9 @@
         either(s == last, gone)
 
     finish()
-    for copies in (az, ax, ac0, ac1, r1, r2, r3):
+    for k in range(sp_count):
+        along_line(k, lambda copy: copy.wait_send())
+    for copies in (ax, ac0, ac1, r1, r2, r3):
         sends.extend(copies.values())
     for copy in sends:
         copy.wait_send()
@@ -615,7 +651,7 @@
             dma((n,)),
             dma((n,)),
             dma((n,)),
-            dma((n,)),
+            dma((2, n)),
             dma((n,)),
             dma((n,)),
             dma((n,)),

time: 131 us -> 121 us (0.924)
  Pallas kernels: 129 us -> 119 us
    pallas_call x1, Pallas kernels: 129 us -> 119 us  [one_device(): pl.pallas_call(functools.partial(layer_kernel, n, widths), out_shape=jax....]
where the time goes in v3:
time: 121 us
  Pallas kernels  119 us (98%)
  local copies, waits for them, and re-layouts  1.62 us (1%)
    pallas_call x1, Pallas kernels, one_device(): pl.pallas_call(functools.partial(layer_kernel, n, widths), out_shape=jax....  119 us

profile of v3, /device:TPU:0, one launch (start us, length us, event | category | flops | bytes accessed | tf_op | source)
XLA Modules:
  0.0 121.1 jit_solution(9894425223112592777)
XLA Ops:
  0.0 119.5 %shard_map.118 = bf16[192,512]{1,0:T(8,128)(2,1)} custom-call(bf16[192,128]{1,0:T(8,128)(2,1)} %q1_ref.1, bf16[192,256]{1,0:T(8,128)(2,1)} %q2_ref.1, bf16[192,128]{1,0:T(8,128)(2,1)} %k1_ref.1, bf16[192,256]{1,0:T(8,128)(2,1)} %k2_ref.1, bf16[192,2,128]{2,1,0:T(2,128)(2,1)} %v_ref.1, f32[1,2]{1,0:T(1,128)} %bitcast.1, bf16[192,512]{1,0:T(8,128)(2,1)} %residual_ref.1, ...), custom_call_target="tpu_custom_call" | custom-call | tf_op jit(solution)/shard_map/pallas_call | solution.py:614
  119.5 1.6 %copy.14 = bf16[192,512]{1,0:T(8,128)(2,1)} copy(bf16[192,512]{1,0:T(8,128)(2,1)} %shard_map.118) | data formatting | bytes 393216
